TPU v7x, 128 devices: a whole 4x4x4 slice. The times are simulated.
128 devices in a mesh: sp: 16 (over z, y), tp: 8 (over x, core).
Axes of the slice: x: 4, y: 4, z: 4, core: 2. Of those that a mesh axis runs over, the one named last changes fastest.
Arguments:
- inputs: bfloat16 [8192, 4096], P(('sp', 'tp')), may hold values from -42 to 42
- a_query_w: bfloat16 [4096, 2048], P(None, 'tp'), may hold values from -0.12570312 to 0.12570312
- a_key_w: bfloat16 [4096, 2048], P(None, 'tp'), may hold values from -0.12570312 to 0.12570312
- a_value_w: bfloat16 [4096, 2048], P(None, 'tp'), may hold values from -0.09375 to 0.09375
- b_query_w: bfloat16 [4096, 2048], P(None, 'tp'), may hold values from -0.12570312 to 0.12570312
- b_key_w: bfloat16 [4096, 512], P(None, 'tp'), may hold values from -0.12570312 to 0.12570312
- b_value_w: bfloat16 [4096, 512], P(None, 'tp'), may hold values from -0.09375 to 0.09375
- head_lambda: float32 [16], P('tp'), may hold values from 0.3 to 0.8
- head_gain: float32 [128], replicated, may hold values from 0.1 to 1.9
- sink_logit: float32 [32], P('tp'), may hold values from 2 to 7
- a_out_w: bfloat16 [2048, 4096], P('tp'), may hold values from -0.125 to 0.125
- b_out_w: bfloat16 [2048, 4096], P('tp'), may hold values from -0.625 to 0.625
Outputs:
- mixed: bfloat16 [8192, 4096], P(('sp', 'tp'))
All inputs are finite; a program needn't handle non-finite values.
Results may differ from a plain program's by a relative error of at most 0.015.
Values may be sent and summed in bfloat16 or wider, within the bound.
A program may use at most 128 MiB of HBM per device.

v0:
```python
import math
import jax
import jax.numpy as jnp
from jax import lax
from jax.sharding import PartitionSpec as P

HEAD_DIM = 64
VALUE_DIM = 128
WINDOW = 128
norm_eps = 0.0001
head_scale = 0.8
mask_fill = -1e30


def from_behind(value, axis, by):
    size = lax.axis_size(axis)
    pairs = [(i, i + by) for i in range(size) if 0 <= i + by < size]
    return lax.ppermute(value, axis, pairs)


def side_by_side(arrays, axis, dim, along):
    widths = [a.shape[along] for a in arrays]
    both = jnp.concatenate(arrays, axis=along)
    whole = lax.all_gather(both, axis, axis=dim, tiled=True)
    return tuple(jnp.split(whole, [sum(widths[:k]) for k in range(1, len(widths))], axis=along))


def key_span(row_count):
    span_rows = math.gcd(row_count, 1024)
    return span_rows


def attend_block(carried, queries, query_pos, block_keys, block_values, key_pos):
    running, totals, numerator = carried
    scores = jnp.einsum(
        "qhmd,khmd->hmqk", queries, block_keys, preferred_element_type=jnp.float32
    ) * HEAD_DIM ** (-0.5)
    allowed = query_pos[:, None] >= key_pos[None, :]
    scores = jnp.where(allowed, scores, mask_fill)
    updated = jnp.maximum(running, jnp.max(scores, axis=-1))
    weights = jnp.where(allowed, jnp.exp(scores - updated[..., None]), 0.0)
    shrink = jnp.exp(running - updated)
    totals = totals * shrink + jnp.sum(weights, axis=-1)
    numerator = numerator * shrink[..., None] + jnp.einsum(
        "hmqk,khe->hmqe",
        weights.astype(jnp.bfloat16),
        block_values,
        preferred_element_type=jnp.float32,
    )
    return (updated, totals, numerator)


def advance(states, groups, key_rows, value_rows):
    row_count = key_rows.shape[0]
    span_rows = key_span(row_count)
    local_heads = value_rows.shape[1] // VALUE_DIM
    key_rows = key_rows.reshape(row_count, local_heads, 2, HEAD_DIM)
    value_rows = value_rows.reshape(row_count, local_heads, VALUE_DIM)

    def one_span(span_index, current):
        span_start = span_index * span_rows
        block_keys = lax.dynamic_slice_in_dim(key_rows, span_start, span_rows, 0)
        block_values = lax.dynamic_slice_in_dim(value_rows, span_start, span_rows, 0)
        key_pos = span_start + jnp.arange(span_rows, dtype=jnp.int32)
        results = []
        for query_group, carried in zip(groups, current):
            queries, query_pos = query_group

            def compute(given_state, queries=queries, query_pos=query_pos):
                return attend_block(
                    given_state, queries, query_pos, block_keys, block_values, key_pos
                )

            def unchanged(given_state):
                return given_state

            results.append(lax.cond(key_pos[0] <= query_pos[-1], compute, unchanged, carried))
        return tuple(results)

    return lax.fori_loop(0, row_count // span_rows, one_span, states)


def finish_heads(carried, head_lambda, head_gain):
    running, totals, numerator = carried
    means = numerator / totals[..., None]
    difference = means[:, 0] - head_lambda[:, None, None] * means[:, 1]
    mean_square = jnp.mean(difference * difference, axis=-1, keepdims=True)
    return (difference * lax.rsqrt(mean_square + norm_eps) * head_gain * head_scale).astype(
        jnp.bfloat16
    )


def shards(
    inputs,
    a_query_w,
    a_key_w,
    a_value_w,
    b_query_w,
    b_key_w,
    b_value_w,
    head_lambda,
    head_gain,
    sink_logit,
    a_out_w,
    b_out_w,
):
    matrices = (a_query_w, a_key_w, a_value_w, b_query_w, b_key_w, b_value_w)

    def project(shard_piece):
        return jnp.concatenate(
            [
                jnp.dot(shard_piece, matrix, preferred_element_type=jnp.float32).astype(
                    jnp.bfloat16
                )
                for matrix in matrices
            ],
            axis=1,
        )

    projected = project(lax.all_gather(inputs, "tp", axis=0, tiled=True))
    seg_rows = projected.shape[0]
    column_edges = [0]
    for matrix in matrices:
        column_edges.append(column_edges[-1] + matrix.shape[1])
    a_query = projected[:, column_edges[0] : column_edges[1]]
    a_key = projected[:, column_edges[1] : column_edges[2]]
    a_value = projected[:, column_edges[2] : column_edges[3]]
    b_query = projected[:, column_edges[3] : column_edges[4]]
    b_pair = projected[:, column_edges[4] : column_edges[6]]
    local_heads = head_lambda.shape[0]
    offset = lax.axis_index("sp") * seg_rows
    positions = offset + jnp.arange(seg_rows, dtype=jnp.int32)
    query_heads = a_query.reshape(seg_rows, local_heads, 2, HEAD_DIM)
    groups = ((query_heads, positions),)
    initial = tuple(
        (
            (
                jnp.full((local_heads, 2, group_queries.shape[0]), mask_fill, jnp.float32),
                jnp.zeros((local_heads, 2, group_queries.shape[0]), jnp.float32),
                jnp.zeros((local_heads, 2, group_queries.shape[0], VALUE_DIM), jnp.float32),
            )
            for group_queries, group_pos in groups
        )
    )
    earlier = from_behind(b_pair[seg_rows - WINDOW :], "sp", 1)
    shard_piece = side_by_side((a_key, a_value), "sp", 0, 1)
    states = advance(initial, groups, shard_piece[0], shard_piece[1])
    finished = [finish_heads(carried, head_lambda, head_gain) for carried in states]
    a_heads = finished[0]
    kv_heads = b_pair.shape[1] // (2 * HEAD_DIM)
    group_size = b_query.shape[1] // HEAD_DIM // kv_heads
    extended = jnp.concatenate([earlier, b_pair], axis=0)
    near_keys = extended[:, : kv_heads * HEAD_DIM].reshape(WINDOW + seg_rows, kv_heads, HEAD_DIM)
    near_values = extended[:, kv_heads * HEAD_DIM :].reshape(WINDOW + seg_rows, kv_heads, HEAD_DIM)
    window_queries = b_query.reshape(seg_rows, kv_heads, group_size, HEAD_DIM)
    sink_term = sink_logit.reshape(kv_heads, group_size)[:, :, None]
    query_span = math.gcd(seg_rows, 512)
    scores = jnp.einsum(
        "qhgd,khd->hgqk", window_queries, near_keys, preferred_element_type=jnp.float32
    ) * HEAD_DIM ** (-0.5)
    query_pos = offset + 0 + jnp.arange(query_span, dtype=jnp.int32)
    near_pos = offset + 0 - WINDOW + jnp.arange(query_span + WINDOW, dtype=jnp.int32)
    distance = query_pos[:, None] - near_pos[None, :]
    allowed = (distance >= 0) & (distance < WINDOW) & (near_pos[None, :] >= 0)
    scores = jnp.where(allowed, scores, mask_fill)
    row_top = jnp.maximum(jnp.max(scores, axis=-1), sink_term)
    weights = jnp.where(allowed, jnp.exp(scores - row_top[..., None]), 0.0)
    row_total = jnp.sum(weights, axis=-1) + jnp.exp(sink_term - row_top)
    probs = (weights / row_total[..., None]).astype(jnp.bfloat16)
    block_out = jnp.einsum("hgqk,khd->qhgd", probs, near_values, preferred_element_type=jnp.float32)
    outputs = block_out.astype(jnp.bfloat16).reshape(query_span, kv_heads * group_size * HEAD_DIM)
    a_weight = a_out_w.reshape(local_heads, VALUE_DIM, a_out_w.shape[1])
    return lax.psum_scatter(
        (
            jnp.einsum("hqe,hen->qn", a_heads, a_weight, preferred_element_type=jnp.float32)
            + jnp.dot(outputs, b_out_w, preferred_element_type=jnp.float32)
        ).astype(jnp.bfloat16),
        "tp",
        scatter_dimension=0,
        tiled=True,
    )


def solution(mesh):
    return jax.shard_map(
        shards,
        mesh=mesh,
        in_specs=(
            P(("sp", "tp"), None),
            P(None, "tp"),
            P(None, "tp"),
            P(None, "tp"),
            P(None, "tp"),
            P(None, "tp"),
            P(None, "tp"),
            P("tp"),
            P(),
            P("tp"),
            P("tp", None),
            P("tp", None),
        ),
        out_specs=P(("sp", "tp"), None),
        check_vma=False,
    )
```

profile of v0, /device:TPU:0, one launch (start us, length us, event | category | flops | bytes accessed | tf_op | source)
XLA Modules:
  0.0 288.8 jit_solution(3257539258130049300)
XLA Ops:
  6.5 0.7 all-gather.3.cloned.1.call-update
  7.3 36.3 %all-gather.3.cloned.1.call-done = bf16[512,4096]{1,0:T(8,128)(2,1)} async-done(((bf16[64,4096]{1,0:T(8,128)(2,1)}), bf16[512,4096]{1,0:T(8,128)(2,1)}) %all-gather.3.cloned.1.call-update) | async-done | bytes 4194320 | tf_op jit(solution)/shard_map/all_gather | solution.py:120
  43.6 4.3 %convolution_convert_fusion.2 = bf16[512,256]{0,1:T(8,128)(2,1)S(1)} fusion(bf16[512,4096]{1,0:T(8,128)(2,1)} %all-gather.3.cloned.1.call-done, bf16[4096,256]{1,0:T(8,128)(2,1)} %param.19), kind=kOutput, calls=%fused_computation.37 | convolution fusion | flops 1073872896 | bytes 6553600 | tf_op jit(solution)/shard_map/dot_general | solution.py:112
  48.3 1.3 convolution_convert_fusion.3
  49.6 0.8 pad_maximum_fusion
  51.0 3.8 %convolution_convert_fusion.4 = bf16[512,64]{0,1:T(8,128)(2,1)S(1)} fusion(bf16[512,4096]{1,0:T(8,128)(2,1)} %all-gather.3.cloned.1.call-done, bf16[4096,64]{0,1:T(8,128)(2,1)S(1)} %copy-done.4), kind=kOutput, calls=%fused_computation.39 | convolution fusion | flops 268468224 | bytes 4784128 | tf_op jit(solution)/shard_map/dot_general | solution.py:112
  54.9 1.4 convolution_convert_fusion.5
  56.3 3.5 %collective-permute-start = (bf16[128,128]{0,1:T(8,128)(2,1)S(1)}, bf16[128,128]{0,1:T(8,128)(2,1)S(1)}, u32[]{:S(2)}, u32[]{:S(2)}) collective-permute-start(bf16[128,128]{0,1:T(8,128)(2,1)S(1)} %pad_maximum_fusion.1), channel_id=1, source_target_pairs={{0,8},{8,16},{16,24},{24,32},{32,40},{40,48},{48,56},{56,64},{64,7... | collective-permute-start | bytes 98312 | tf_op jit(solution)/shard_map/ppermute | solution.py:18
  59.8 1.3 convolution_convert_fusion
  61.2 2.0 convolution_convert_fusion.1
  63.2 1.0 fusion.19
  64.3 1.3 fusion.20
  65.7 1.8 fusion.25
  67.6 60.4 %all-gather.5.cloned.1.call-done = bf16[8192,512]{0,1:T(8,128)(2,1)} async-done(((bf16[512,512]{0,1:T(8,128)(2,1)}), bf16[8192,512]{0,1:T(8,128)(2,1)}) %all-gather.5.cloned.1.call-update) | async-done | bytes 8388624 | tf_op jit(solution)/shard_map/all_gather | solution.py:24
  128.0 5.9 %fusion.40 = (bf16[8192,256]{0,1:T(8,128)(2,1)}, bf16[8192,256]{0,1:T(8,128)(2,1)}) fusion(bf16[8192,512]{0,1:T(8,128)(2,1)} %all-gather.5.cloned.1.call-done), kind=kLoop, calls=%fused_computation.68 | loop fusion | bytes 16777216 | tf_op jit(solution)/shard_map/split | solution.py:25
  133.9 6.3 %copy.14 = bf16[8192,2,128]{2,0,1:T(8,128)(2,1)} copy(bf16[8192,2,128]{0,2,1:T(8,128)(2,1)} %bitcast.105) | data formatting | bytes 8388608 | tf_op jit(solution)/shard_map/while | solution.py:80
  140.3 31.0 %while.17 = (s32[]{:T(128)}, f32[2,2,512]{2,1,0:T(2,128)S(1)}, f32[2,2,512]{2,1,0:T(2,128)S(1)}, f32[2,2,512,128]{3,2,1,0:T(8,128)S(1)}, s32[512]{0:T(512)S(1)},...) while((s32[]{:T(128)}, f32[2,2,512]{2,1,0:T(2,128)S(1)}, ...), condition=%wide.region_5.6_spmd, body=%wide.region_0.5_spmd.sunk | while | flops 833623040 | bytes 30812476 | solution.py:80
  140.3 0.6 slice.65
  142.9 9.8 %conditional.2 = ((f32[2,2,512]{2,1,0:T(2,128)S(1)}, f32[2,2,512]{2,1,0:T(2,128)S(1)}, f32[2,2,512,128]{3,2,1,0:T(8,128)S(1)})) conditional(s32[]{:T(128)} %bitcast.103, (f32[2,2,512]{2,1,0:T(2,128)S(1)}, f32[2,2,512]{2,1,0:T(2,128)S(1)}, f32[2,2,512,128]{3,2,1,0:T(8,128)S(1)}) %tuple.51, (s32[512]{0:T(512)S(1)}, s32[1024]{0:T(1024)S(1)}, s32[]{:T(128)}, ...), branch_computations={%region_1.0_spmd, %region_2.4_spmd} | conditional | flops 833622016 | bytes 30808138 | solution.py:77
  143.3 2.7 fusion
  146.1 2.1 fusion.2
  148.2 4.5 %fusion.6 = f32[2,2,512,128]{3,2,1,0:T(8,128)S(1)} fusion(f32[2,2,1024,512]{3,2,1,0:T(8,128)S(1)} %get-tuple-element.290, f32[2,2,512]{2,1,0:T(2,128)S(1)} %max.21, pred[512,1024]{0,1:T(8,128)(4,1)S(1)} %broadcast_compare_fusion, f32[2,2,512,128]{3,2,1,0:T(8,128)S(1)} %get-tuple-element.245, bf16[8192,2,128]{2,0,1:T(8,128)(2,1)} %get-tuple-element.246, ...), kind=kOutput, calls=%fused_computation.7 | convolution fusion | flops 547880960 | bytes 11550724 | tf_op jit(solution)/shard_map/while/body/eval_jaxpr/cond/branch_1_fun/hmqk,khe->hmqe/dot_general | solution.py:44
  152.7 0.6 slice.65
  155.4 0.6 slice.65
  158.1 0.6 slice.65
  160.7 0.6 slice.65
  163.4 0.6 slice.65
  166.0 0.6 slice.65
  168.7 0.6 slice.65
  172.0 1.3 fusion.30
  173.6 3.3 %fusion.18 = bf16[512,4096]{1,0:T(8,128)(2,1)} fusion(f32[512,4096,1]{1,0,2:T(8,128)S(1)} %fusion.30, bf16[512,256]{0,1:T(8,128)(2,1)S(1)} %bitcast.107, bf16[256,4096]{1,0:T(8,128)(2,1)S(1)} %copy-done.3), kind=kOutput, calls=%fused_computation.22 | convolution fusion | flops 1077936128 | bytes 14942208 | tf_op jit(solution)/shard_map/dot_general | solution.py:176
  176.9 105.4 %reduce-scatter.2.cloned.1.call-done = bf16[64,4096]{1,0:T(8,128)(2,1)} async-done(((bf16[512,4096]{1,0:T(8,128)(2,1)}), bf16[64,4096]{1,0:T(8,128)(2,1)}) %reduce-scatter.2.cloned.1.call-update) | async-done | bytes 524304 | tf_op jit(solution)/shard_map/reduce_scatter | solution.py:173
  (71 shorter events, 7.4 us)
Async XLA Ops:
  6.5 165.5 %copy-start = (bf16[256,4096]{1,0:T(8,128)(2,1)S(1)}, bf16[256,4096]{1,0:T(8,128)(2,1)}, u32[]{:S(2)}) copy-start(bf16[256,4096]{1,0:T(8,128)(2,1)} %param.26) | copy-start | bytes 6291460
  6.5 37.0 %all-gather.3.cloned.1.call-start = ((), (), s32[]{:S(2)}) async-start(), calls=%async_computation.1 | async-start | bytes 4718592 | tf_op jit(solution)/shard_map/all_gather | solution.py:120
  7.3 120.7 %all-gather.5.cloned.1.call-start = ((), (), s32[]{:S(2)}) async-start(), calls=%async_computation.2 | async-start | bytes 8912896 | tf_op jit(solution)/shard_map/all_gather | solution.py:24
  43.6 4.3 %copy-start.1 = (bf16[512,4096]{1,0:T(8,128)(2,1)S(1)}, bf16[512,4096]{1,0:T(8,128)(2,1)}, u32[]{:S(2)}) copy-start(bf16[512,4096]{1,0:T(8,128)(2,1)} %all-gather.3.cloned.1.call-done) | copy-start | bytes 12582916
  43.6 4.7 %copy-start.9 = (bf16[4096,256]{1,0:T(8,128)(2,1)S(1)}, bf16[4096,256]{1,0:T(8,128)(2,1)}, u32[]{:S(2)}) copy-start(bf16[4096,256]{1,0:T(8,128)(2,1)} %param.18) | copy-start | bytes 6291460
  48.3 2.7 copy-start.4
  49.6 5.2 %copy-start.5 = (bf16[4096,64]{0,1:T(8,128)(2,1)S(1)}, bf16[4096,64]{0,1:T(8,128)(2,1)}, u32[]{:S(2)}) copy-start(bf16[4096,64]{0,1:T(8,128)(2,1)} %param.21) | copy-start | bytes 1572868
  50.5 231.8 %reduce-scatter.2.cloned.1.call-start = ((), (), s32[]{:S(2)}) async-start(), calls=%async_computation.3 | async-start | bytes 4718592 | tf_op jit(solution)/shard_map/reduce_scatter | solution.py:173
  50.5 4.3 %copy-start.2 = (bf16[512,4096]{1,0:T(8,128)(2,1)S(1)}, bf16[512,4096]{1,0:T(8,128)(2,1)}, u32[]{:S(2)}) copy-start(bf16[512,4096]{1,0:T(8,128)(2,1)} %all-gather.3.cloned.1.call-done) | copy-start | bytes 12582916
  51.0 8.8 %copy-start.10 = (bf16[4096,256]{1,0:T(8,128)(2,1)S(1)}, bf16[4096,256]{1,0:T(8,128)(2,1)}, u32[]{:S(2)}) copy-start(bf16[4096,256]{1,0:T(8,128)(2,1)} %param.20) | copy-start | bytes 6291460
  56.3 4.9 %copy-start.11 = (bf16[4096,256]{1,0:T(8,128)(2,1)S(1)}, bf16[4096,256]{1,0:T(8,128)(2,1)}, u32[]{:S(2)}) copy-start(bf16[4096,256]{1,0:T(8,128)(2,1)} %param.17) | copy-start | bytes 6291460
  56.3 6.9 %collective-permute-start = (bf16[128,128]{0,1:T(8,128)(2,1)S(1)}, bf16[128,128]{0,1:T(8,128)(2,1)S(1)}, u32[]{:S(2)}, u32[]{:S(2)}) collective-permute-start(bf16[128,128]{0,1:T(8,128)(2,1)S(1)} %pad_maximum_fusion.1), channel_id=1, source_target_pairs={{0,8},{8,16},{16,24},{24,32},{32,40},{40,48},{48,56},{56,64},{64,7... | collective-permute-start | bytes 98312 | tf_op jit(solution)/shard_map/ppermute | solution.py:18
  63.2 1.1 copy-start.8
  140.3 31.4 %copy-start.6 = (f32[2]{0:T(128)S(1)}, f32[2]{0:T(128)}, u32[]{:S(2)}) copy-start(f32[2]{0:T(128)} %param.23) | copy-start | bytes 28
  140.3 31.7 %copy-start.7 = (f32[128]{0:T(128)S(1)}, f32[128]{0:T(128)}, u32[]{:S(2)}) copy-start(f32[128]{0:T(128)} %param.24) | copy-start | bytes 1540
  172.0 1.6 copy-start.3
Sparse Core Ops, SparseCore 0:
  9.0 34.4 all-gather.2
  50.6 77.3 all-gather.4
  177.0 105.1 reduce-scatter.1
where the time goes:
time: 290 us; the launch traced here: 289 us
  waiting for transfers between devices  203 us (70%)
  matrix products  28.8 us (10%)
  local copies, waits for them, and re-layouts  23 us (8%)
  between operations  13.4 us (5%)
  loops' own time  11.3 us (4%)
  other arithmetic  5.89 us (2%)
  starting transfers between devices  3.61 us (1%)
    reduce_scatter x1, waiting for transfers between devices, shards(): lax.psum_scatter((jnp.einsum('hqe,hen->qn', a_heads, a_weight, preferred_...  105 us
    all_gather x1, waiting for transfers between devices, side_by_side(): whole = lax.all_gather(both, axis, axis=dim, tiled=True)  60.4 us
    all_gather x1, waiting for transfers between devices, shards(): projected = project(lax.all_gather(inputs, 'tp', axis=0, tiled=True))  36.3 us
    dot_general x6, matrix products, project(): jnp.dot(shard_piece, matrix, preferred_element_type=jnp.float32)  14.1 us
    another operation x1, loops' own time, advance(): return lax.fori_loop(0, row_count // span_rows, one_span, states)  11.2 us
    while x1, local copies, waits for them, and re-layouts, advance(): return lax.fori_loop(0, row_count // span_rows, one_span, states)  6.32 us
    split x1, local copies, waits for them, and re-layouts, side_by_side(): jnp.split(whole, [sum(widths[:k]) for k in range(1, len(widths))], axis=a...  5.86 us
  transfers between devices with their start and end apart: 4, of which 3 were waited for; matrix products, arithmetic and copies ran while one was open for 5% of the time, Pallas kernels for 0%

commit v1 on v0

--- a/solution.py
+++ b/solution.py
@@ -117,7 +117,11 @@
             axis=1,
         )
 
-    projected = project(lax.all_gather(inputs, "tp", axis=0, tiled=True))
+    projected = project(
+        jnp.concatenate(
+            lax.all_to_all(jnp.stack([inputs] * lax.axis_size("tp")), "tp", 0, 0), axis=0
+        )
+    )
     seg_rows = projected.shape[0]
     column_edges = [0]
     for matrix in matrices:

time: 290 us -> 306 us (1.055)
  blocking collectives: 0 us -> 54 us
  waiting for transfers between devices: 203 us -> 166 us
    all_to_all x0 -> x1, blocking collectives: none -> 54 us  [shards(): lax.all_to_all(jnp.stack([inputs] * lax.axis_size('tp')), 'tp', 0, 0)]
    all_gather x1 -> x0, waiting for transfers between devices: 36.3 us -> none  [shards(): projected = project(lax.all_gather(inputs, 'tp', axis=0, tiled=True))]
  transfers between devices with their start and end apart: 4 -> 3, of which waited for: 3 -> 2; matrix products, arithmetic and copies ran while one was open for 5% -> 4% of each run, Pallas kernels for 0% -> 0%
where the time goes in v1:
time: 306 us; the launch traced here: 305 us
  waiting for transfers between devices  166 us (54%)
  blocking collectives  54 us (18%)
  matrix products  25.8 us (8%)
  local copies, waits for them, and re-layouts  25.5 us (8%)
  between operations  13.7 us (4%)
  loops' own time  10.4 us (3%)
  other arithmetic  5.89 us (2%)
  starting transfers between devices  3.84 us (1%)
    reduce_scatter x1, waiting for transfers between devices, shards(): lax.psum_scatter((jnp.einsum('hqe,hen->qn', a_heads, a_weight, preferred_...  105 us
    all_gather x1, waiting for transfers between devices, side_by_side(): whole = lax.all_gather(both, axis, axis=dim, tiled=True)  60.7 us
    all_to_all x1, blocking collectives, shards(): lax.all_to_all(jnp.stack([inputs] * lax.axis_size('tp')), 'tp', 0, 0)  54 us
    dot_general x6, matrix products, project(): jnp.dot(shard_piece, matrix, preferred_element_type=jnp.float32)  11.1 us
    another operation x1, loops' own time, advance(): return lax.fori_loop(0, row_count // span_rows, one_span, states)  10.3 us
    while x1, local copies, waits for them, and re-layouts, advance(): return lax.fori_loop(0, row_count // span_rows, one_span, states)  6.32 us
  transfers between devices with their start and end apart: 3, of which 2 were waited for; matrix products, arithmetic and copies ran while one was open for 4% of the time, Pallas kernels for 0%

profile of v1, /device:TPU:0, one launch (start us, length us, event | category | flops | bytes accessed | tf_op | source)
XLA Modules:
  0.0 305.1 jit_solution(1268076111377155211)
XLA Ops:
  6.5 1.7 stack.2
  8.2 54.0 %all_to_all.5 = bf16[8,64,4096]{2,1,0:T(8,128)(2,1)S(1)} all-to-all(bf16[8,64,4096]{2,1,0:T(8,128)(2,1)S(1)} %stack.2), channel_id=1, replica_groups=mesh['sp'=16,'tp'=8] {'tp'}, dimensions={0} | all-to-all | bytes 8388608 | tf_op jit(solution)/shard_map/all_to_all | solution.py:122
  62.3 1.3 convolution_convert_fusion.2
  63.6 0.8 copy-done.1
  64.4 1.0 copy-done.10
  65.4 1.3 convolution_convert_fusion.3
  66.7 0.8 pad_maximum_fusion
  68.1 3.8 %convolution_convert_fusion.4 = bf16[512,64]{0,1:T(8,128)(2,1)S(1)} fusion(bf16[512,4096]{1,0:T(8,128)(2,1)} %bitcast.108, bf16[4096,64]{0,1:T(8,128)(2,1)S(1)} %copy-done.4), kind=kOutput, calls=%fused_computation.39 | convolution fusion | flops 268468224 | bytes 4784128 | tf_op jit(solution)/shard_map/dot_general | solution.py:112
  71.9 1.4 convolution_convert_fusion.5
  73.4 3.8 %collective-permute-start = (bf16[128,128]{0,1:T(8,128)(2,1)S(1)}, bf16[128,128]{0,1:T(8,128)(2,1)S(1)}, u32[]{:S(2)}, u32[]{:S(2)}) collective-permute-start(bf16[128,128]{0,1:T(8,128)(2,1)S(1)} %pad_maximum_fusion.1), channel_id=1, source_target_pairs={{0,8},{8,16},{16,24},{24,32},{32,40},{40,48},{48,56},{56,64},{64,7... | collective-permute-start | bytes 98312 | tf_op jit(solution)/shard_map/ppermute | solution.py:18
  77.2 1.3 convolution_convert_fusion
  78.5 2.0 convolution_convert_fusion.1
  80.5 1.0 fusion.19
  81.7 1.3 fusion.20
  83.0 1.8 fusion.25
  84.9 60.7 %all-gather.2.cloned.1.call-done = bf16[8192,512]{0,1:T(8,128)(2,1)} async-done(((bf16[512,512]{0,1:T(8,128)(2,1)}), bf16[8192,512]{0,1:T(8,128)(2,1)}) %all-gather.2.cloned.1.call-update) | async-done | bytes 8388624 | tf_op jit(solution)/shard_map/all_gather | solution.py:24
  145.6 5.9 %fusion.40 = (bf16[8192,256]{0,1:T(8,128)(2,1)}, bf16[8192,256]{0,1:T(8,128)(2,1)}) fusion(bf16[8192,512]{0,1:T(8,128)(2,1)} %all-gather.2.cloned.1.call-done), kind=kLoop, calls=%fused_computation.68 | loop fusion | bytes 16777216 | tf_op jit(solution)/shard_map/split | solution.py:25
  151.5 6.3 %copy.14 = bf16[8192,2,128]{2,0,1:T(8,128)(2,1)} copy(bf16[8192,2,128]{0,2,1:T(8,128)(2,1)} %bitcast.112) | data formatting | bytes 8388608 | tf_op jit(solution)/shard_map/while | solution.py:80
  157.9 29.5 %while.17 = (s32[]{:T(128)}, f32[2,2,512]{2,1,0:T(2,128)S(1)}, f32[2,2,512]{2,1,0:T(2,128)S(1)}, f32[2,2,512,128]{3,2,1,0:T(8,128)S(1)}, s32[512]{0:T(512)S(1)},...) while((s32[]{:T(128)}, f32[2,2,512]{2,1,0:T(2,128)S(1)}, ...), condition=%wide.region_5.6_spmd, body=%wide.region_0.5_spmd.sunk | while | flops 833623040 | bytes 30812476 | solution.py:80
  157.9 0.6 slice.65
  160.3 9.8 %conditional.2 = ((f32[2,2,512]{2,1,0:T(2,128)S(1)}, f32[2,2,512]{2,1,0:T(2,128)S(1)}, f32[2,2,512,128]{3,2,1,0:T(8,128)S(1)})) conditional(s32[]{:T(128)} %bitcast.104, (f32[2,2,512]{2,1,0:T(2,128)S(1)}, f32[2,2,512]{2,1,0:T(2,128)S(1)}, f32[2,2,512,128]{3,2,1,0:T(8,128)S(1)}) %tuple.51, (s32[512]{0:T(512)S(1)}, s32[1024]{0:T(1024)S(1)}, s32[]{:T(128)}, ...), branch_computations={%region_1.0_spmd, %region_2.4_spmd} | conditional | flops 833622016 | bytes 30808138 | solution.py:77
  160.7 2.7 fusion
  163.5 2.1 fusion.2
  165.6 4.5 %fusion.6 = f32[2,2,512,128]{3,2,1,0:T(8,128)S(1)} fusion(f32[2,2,1024,512]{3,2,1,0:T(8,128)S(1)} %get-tuple-element.290, f32[2,2,512]{2,1,0:T(2,128)S(1)} %max.21, pred[512,1024]{0,1:T(8,128)(4,1)S(1)} %broadcast_compare_fusion, f32[2,2,512,128]{3,2,1,0:T(8,128)S(1)} %get-tuple-element.245, bf16[8192,2,128]{2,0,1:T(8,128)(2,1)} %get-tuple-element.246, ...), kind=kOutput, calls=%fused_computation.7 | convolution fusion | flops 547880960 | bytes 11550724 | tf_op jit(solution)/shard_map/while/body/eval_jaxpr/cond/branch_1_fun/hmqk,khe->hmqe/dot_general | solution.py:44
  170.1 0.6 slice.65
  172.6 0.6 slice.65
  175.1 0.6 slice.65
  180.0 0.6 slice.65
  184.9 0.6 slice.65
  188.1 1.3 fusion.30
  189.7 3.3 %fusion.18 = bf16[512,4096]{1,0:T(8,128)(2,1)} fusion(f32[512,4096,1]{1,0,2:T(8,128)S(1)} %fusion.30, bf16[512,256]{0,1:T(8,128)(2,1)S(1)} %bitcast.114, bf16[256,4096]{1,0:T(8,128)(2,1)S(1)} %copy-done.3), kind=kOutput, calls=%fused_computation.22 | convolution fusion | flops 1077936128 | bytes 14942208 | tf_op jit(solution)/shard_map/dot_general | solution.py:180
  192.9 105.3 %reduce-scatter.2.cloned.1.call-done = bf16[64,4096]{1,0:T(8,128)(2,1)} async-done(((bf16[512,4096]{1,0:T(8,128)(2,1)}), bf16[64,4096]{1,0:T(8,128)(2,1)}) %reduce-scatter.2.cloned.1.call-update) | async-done | bytes 524304 | tf_op jit(solution)/shard_map/reduce_scatter | solution.py:177
  (72 shorter events, 8.0 us)
Async XLA Ops:
  6.5 181.5 %copy-start = (bf16[256,4096]{1,0:T(8,128)(2,1)S(1)}, bf16[256,4096]{1,0:T(8,128)(2,1)}, u32[]{:S(2)}) copy-start(bf16[256,4096]{1,0:T(8,128)(2,1)} %param.26) | copy-start | bytes 6291460
  6.5 139.0 %all-gather.2.cloned.1.call-start = ((), (), s32[]{:S(2)}) async-start(), calls=%async_computation.2 | async-start | bytes 8912896 | tf_op jit(solution)/shard_map/all_gather | solution.py:24
  8.2 54.0 %copy-start.9 = (bf16[4096,256]{1,0:T(8,128)(2,1)S(1)}, bf16[4096,256]{1,0:T(8,128)(2,1)}, u32[]{:S(2)}) copy-start(bf16[4096,256]{1,0:T(8,128)(2,1)} %param.19) | copy-start | bytes 6291460
  62.3 2.1 copy-start.1
  62.3 3.1 %copy-start.10 = (bf16[4096,256]{1,0:T(8,128)(2,1)S(1)}, bf16[4096,256]{1,0:T(8,128)(2,1)}, u32[]{:S(2)}) copy-start(bf16[4096,256]{1,0:T(8,128)(2,1)} %param.18) | copy-start | bytes 6291460
  65.4 2.7 copy-start.4
  66.7 5.2 %copy-start.5 = (bf16[4096,64]{0,1:T(8,128)(2,1)S(1)}, bf16[4096,64]{0,1:T(8,128)(2,1)}, u32[]{:S(2)}) copy-start(bf16[4096,64]{0,1:T(8,128)(2,1)} %param.21) | copy-start | bytes 1572868
  67.5 230.7 %reduce-scatter.2.cloned.1.call-start = ((), (), s32[]{:S(2)}) async-start(), calls=%async_computation.3 | async-start | bytes 4718592 | tf_op jit(solution)/shard_map/reduce_scatter | solution.py:177
  67.6 4.3 %copy-start.2 = (bf16[8,64,4096]{2,1,0:T(8,128)(2,1)S(1)}, bf16[8,64,4096]{2,1,0:T(8,128)(2,1)}, u32[]{:S(2)}) copy-start(bf16[8,64,4096]{2,1,0:T(8,128)(2,1)} %copy-done.1) | copy-start | bytes 12582916
  68.1 9.1 %copy-start.11 = (bf16[4096,256]{1,0:T(8,128)(2,1)S(1)}, bf16[4096,256]{1,0:T(8,128)(2,1)}, u32[]{:S(2)}) copy-start(bf16[4096,256]{1,0:T(8,128)(2,1)} %param.20) | copy-start | bytes 6291460
  73.4 5.1 %copy-start.12 = (bf16[4096,256]{1,0:T(8,128)(2,1)S(1)}, bf16[4096,256]{1,0:T(8,128)(2,1)}, u32[]{:S(2)}) copy-start(bf16[4096,256]{1,0:T(8,128)(2,1)} %param.17) | copy-start | bytes 6291460
  73.4 7.1 %collective-permute-start = (bf16[128,128]{0,1:T(8,128)(2,1)S(1)}, bf16[128,128]{0,1:T(8,128)(2,1)S(1)}, u32[]{:S(2)}, u32[]{:S(2)}) collective-permute-start(bf16[128,128]{0,1:T(8,128)(2,1)S(1)} %pad_maximum_fusion.1), channel_id=1, source_target_pairs={{0,8},{8,16},{16,24},{24,32},{32,40},{40,48},{48,56},{56,64},{64,7... | collective-permute-start | bytes 98312 | tf_op jit(solution)/shard_map/ppermute | solution.py:18
  80.5 1.1 copy-start.8
  157.9 29.9 %copy-start.6 = (f32[2]{0:T(128)S(1)}, f32[2]{0:T(128)}, u32[]{:S(2)}) copy-start(f32[2]{0:T(128)} %param.23) | copy-start | bytes 28
  157.9 30.2 %copy-start.7 = (f32[128]{0:T(128)S(1)}, f32[128]{0:T(128)}, u32[]{:S(2)}) copy-start(f32[128]{0:T(128)} %param.24) | copy-start | bytes 1540
  188.1 1.6 copy-start.3
Sparse Core Ops, SparseCore 0:
  67.7 77.8 all-gather.1
  193.1 105.1 reduce-scatter.1
